TPU v7x, 256 devices: a whole 4x4x8 slice. The times are simulated.
256 devices in a mesh: rep: 2 (over z_hi), fs: 16 (over z_lo, x), tp: 8 (over y, core).
Axes of the slice: x: 4, y: 4, z: 8 (z_hi: 2, z_lo: 4; z = z_hi * 4 + z_lo), core: 2. Of those that a mesh axis runs over, the one named last changes fastest.
Arguments:
- stream: bfloat16 [32768, 2048], P(('rep', 'fs', 'tp')), may hold values from -6 to 6
- gate_weight: bfloat16 [2048, 2816], P('fs', 'tp'), may hold values from -0.125 to 0.125
- up_weight: bfloat16 [2048, 2816], P('fs', 'tp'), may hold values from -0.125 to 0.125
- down_weight: bfloat16 [2816, 2048], P('tp', 'fs'), may hold values from -0.21875 to 0.21875
- query_weight: bfloat16 [2048, 512], P('fs', 'tp'), may hold values from -0.125 to 0.125
- key_weight: bfloat16 [2048, 512], P('fs', 'tp'), may hold values from -0.125 to 0.125
- value_weight: bfloat16 [2048, 1024], P('fs', 'tp'), may hold values from -0.125 to 0.125
- outgate_weight: bfloat16 [2048, 1024], P('fs', 'tp'), may hold values from -0.125 to 0.125
- decay_down: bfloat16 [2048, 32], replicated, may hold values from -0.125 to 0.125
- decay_up: bfloat16 [32, 512], P(None, 'tp'), may hold values from -2 to 2
- decay_bias: float32 [512], P('tp'), may hold values from -0.5 to 7
- head_gain: float32 [128], replicated, may hold values from 0.1 to 1.9
- out_weight: bfloat16 [1024, 2048], P('tp', 'fs'), may hold values from -0.375 to 0.375
- norm_gain: float32 [3, 2048], replicated, may hold values from 0.1 to 1.9
Outputs:
- layer_out: bfloat16 [32768, 2048], P(('rep', 'fs', 'tp'))
All inputs are finite; a program needn't handle non-finite values.
Results may differ from a plain program's by a relative error of at most 0.015.
Values may be sent and summed in bfloat16 or wider, within the bound.
A program may use at most 128 MiB of HBM per device.

v0:
```python
import jax
import jax.numpy as jnp
from jax import lax
from jax.sharding import PartitionSpec as P

DK = 64
DV = 128
BLOCK = 64
RESIDUAL_SCALE = 2.0**0.5
BRANCH_SCALE = 0.5
NORM_EPS = 1e-05
HEAD_EPS = 0.01
GATE_DIVISOR = 16.0


def from_everyone(value, axis):
    copies = jnp.broadcast_to(value, (lax.axis_size(axis), *value.shape))
    return lax.all_to_all(copies, axis, split_axis=0, concat_axis=0, tiled=True)


def joined_along(pieces, dim):
    pieces = jnp.moveaxis(pieces, 0, dim)
    lengths = pieces.shape
    return pieces.reshape(*lengths[:dim], lengths[dim] * lengths[dim + 1], *lengths[dim + 2 :])


def gather_directly(value, axis, dim):
    pieces = from_everyone(value, axis)
    return joined_along(pieces, dim)


def side_by_side(arrays, axis, dim, along):
    widths = [a.shape[along] for a in arrays]
    both = jnp.concatenate(arrays, axis=along)
    result = lax.all_gather(both, axis, axis=dim, tiled=True)
    return tuple(jnp.split(result, [sum(widths[:k]) for k in range(1, len(widths))], axis=along))


def layer_norm(values, norm_scale):
    average = jnp.mean(values, -1, keepdims=True)
    centred = values - average
    spread = jnp.mean(centred * centred, -1, keepdims=True)
    return (centred * lax.rsqrt(spread + NORM_EPS) * norm_scale).astype(jnp.bfloat16)


def blocked_mixer(query, key_rows, value_rows, log_gate):
    length, head_count, key_dim = query.shape
    value_dim = value_rows.shape[2]
    block_count = length // BLOCK

    def split_blocks(values):
        return values.reshape(block_count, BLOCK, head_count, values.shape[2]).transpose(0, 2, 1, 3)

    causal = jnp.tril(jnp.ones((BLOCK, BLOCK), dtype=bool))

    def advance(carried, inputs):
        query_blk, key_blk, value_blk, decay_blk = inputs
        log_gaps = decay_blk[:, :, None, :] - decay_blk[:, None, :, :]
        log_gaps = jnp.where(causal[None, :, :, None], log_gaps, -jnp.inf)
        scores = jnp.sum(
            query_blk[:, :, None, :] * key_blk[:, None, :, :] * jnp.exp(log_gaps), axis=-1
        )
        inside = jnp.einsum("hij,hjv->hiv", scores, value_blk)
        carried_part = jnp.einsum("hid,hdv->hiv", query_blk * jnp.exp(decay_blk), carried)
        closing = decay_blk[:, -1, :]
        update = jnp.einsum(
            "hjd,hjv->hdv", key_blk * jnp.exp(closing[:, None, :] - decay_blk), value_blk
        )
        return (carried * jnp.exp(closing)[:, :, None] + update, inside + carried_part)

    cumulative = jnp.cumsum(split_blocks(log_gate), axis=2)
    start_state = jnp.zeros((head_count, key_dim, value_dim), jnp.float32)
    _, outputs = lax.scan(
        advance,
        start_state,
        (split_blocks(query), split_blocks(key_rows), split_blocks(value_rows), cumulative),
    )
    return outputs.transpose(0, 2, 1, 3).reshape(length, head_count, value_dim)


def on_device(
    stream,
    gate_weight,
    up_weight,
    down_weight,
    query_weight,
    key_weight,
    value_weight,
    outgate_weight,
    decay_down,
    decay_up,
    decay_bias,
    head_gain,
    out_weight,
    norm_gain,
):
    down_local = gather_directly(down_weight, "fs", 1)
    down_full = lax.all_gather(down_local, "tp", axis=0, tiled=True)

    def ffn_half(current, norm_scale):
        gathered = lax.all_gather(current, "tp", axis=0, tiled=True)
        pieces = side_by_side((gate_weight, up_weight), "fs", 0, 1)
        gate = jnp.dot(gathered, pieces[0], preferred_element_type=jnp.float32)
        upward = jnp.dot(gathered, pieces[1], preferred_element_type=jnp.float32)
        hidden = (jax.nn.silu(gate) * upward).astype(jnp.bfloat16)
        own_hidden = lax.all_to_all(hidden, "tp", split_axis=0, concat_axis=1, tiled=True)
        summed = jnp.dot(own_hidden, down_full, preferred_element_type=jnp.float32)
        return layer_norm(
            RESIDUAL_SCALE * current.astype(jnp.float32) + BRANCH_SCALE * summed, norm_scale
        )

    first = ffn_half(stream, norm_gain[0])
    gathered = lax.all_gather(first, "tp", axis=0, tiled=True)
    length = gathered.shape[0]
    pieces = side_by_side((query_weight, key_weight, value_weight, outgate_weight), "fs", 0, 1)
    query, key_rows, value_rows, outgate = tuple(
        (jnp.dot(gathered, piece, preferred_element_type=jnp.float32) for piece in pieces)
    )
    query = query.astype(jnp.bfloat16)
    key_rows = key_rows.astype(jnp.bfloat16)
    value_rows = value_rows.astype(jnp.bfloat16)
    outgate = outgate.astype(jnp.bfloat16)
    low_rank = jnp.dot(gathered, decay_down, preferred_element_type=jnp.float32).astype(
        jnp.bfloat16
    )
    pre_gate = jnp.dot(low_rank, decay_up, preferred_element_type=jnp.float32) + decay_bias
    log_gate = jax.nn.log_sigmoid(pre_gate) / GATE_DIVISOR
    local_heads = query.shape[1] // DK
    mixed = blocked_mixer(
        query.astype(jnp.float32).reshape(length, local_heads, DK) * DK ** (-0.5),
        key_rows.astype(jnp.float32).reshape(length, local_heads, DK),
        value_rows.astype(jnp.float32).reshape(length, local_heads, DV),
        log_gate.reshape(length, local_heads, DK),
    )
    normed = mixed * lax.rsqrt(jnp.mean(mixed * mixed, -1, keepdims=True) + HEAD_EPS) * head_gain
    gated = (
        normed.reshape(length, local_heads * DV) * jax.nn.silu(outgate.astype(jnp.float32))
    ).astype(jnp.bfloat16)
    out_local = gather_directly(out_weight, "fs", 1)
    out_full = lax.all_gather(out_local, "tp", axis=0, tiled=True)
    own_gated = lax.all_to_all(gated, "tp", split_axis=0, concat_axis=1, tiled=True)
    summed = jnp.dot(own_gated, out_full, preferred_element_type=jnp.float32)
    second = layer_norm(RESIDUAL_SCALE * first.astype(jnp.float32) + summed, norm_gain[1])
    return ffn_half(second, norm_gain[2])


def solution(mesh):
    in_specs = (
        P(("rep", "fs", "tp"), None),
        P("fs", "tp"),
        P("fs", "tp"),
        P("tp", "fs"),
        P("fs", "tp"),
        P("fs", "tp"),
        P("fs", "tp"),
        P("fs", "tp"),
        P(),
        P(None, "tp"),
        P("tp"),
        P(),
        P("tp", "fs"),
        P(),
    )
    out_specs = P(("rep", "fs", "tp"), None)
    return jax.shard_map(
        on_device, mesh=mesh, in_specs=in_specs, out_specs=out_specs, check_vma=False
    )
```

profile of v0, /device:TPU:1, one launch (start us, length us, event | category | flops | bytes accessed | tf_op | source)
XLA Modules:
  0.0 473.2 jit_solution(7399616951409170826)
XLA Ops:
  10.1 57.1 %all_to_all.67 = bf16[16,352,128]{2,1,0:T(8,128)(2,1)S(1)} all-to-all(bf16[16,352,128]{2,1,0:T(8,128)(2,1)S(1)} %broadcast_in_dim.32), channel_id=1, replica_groups=mesh['rep'=2,'fs'=16,'tp'=8] {'fs'}, dimensions={0} | all-to-all | bytes 2883584 | tf_op jit(solution)/shard_map/all_to_all | solution.py:18
  69.6 27.4 %all-gather.8.cloned.1.call-done = bf16[2048,704]{0,1:T(8,128)(2,1)} async-done(((bf16[128,704]{0,1:T(8,128)(2,1)}), bf16[2048,704]{0,1:T(8,128)(2,1)}) %all-gather.8.cloned.1.call-update) | async-done | bytes 2883600 | tf_op jit(solution)/shard_map/all_gather | solution.py:35
  97.0 44.9 %all-gather.10.cloned.1.call-done = bf16[1024,2048]{1,0:T(8,128)(2,1)} async-done(((bf16[128,2048]{1,0:T(8,128)(2,1)}), bf16[1024,2048]{1,0:T(8,128)(2,1)}) %all-gather.10.cloned.1.call-update) | async-done | bytes 4194320 | tf_op jit(solution)/shard_map/all_gather | solution.py:101
  141.9 4.5 convolution_bitcast_fusion.2
  149.3 3.7 all-to-all-start
  153.1 14.9 %all-to-all-done = bf16[8,128,352]{1,2,0:T(8,128)(2,1)S(1)} async-done(((bf16[8,128,352]{1,2,0:T(8,128)(2,1)}), bf16[8,128,352]{1,2,0:T(8,128)(2,1)S(1)}, u32[]{:S(2)}, u32[]{:S(2)}) %all-to-all-start) | async-done | bytes 720928 | tf_op jit(solution)/shard_map/all_to_all | solution.py:106
  168.0 45.3 %all-gather.12.cloned.1.call-done = bf16[2816,2048]{1,0:T(8,128)(2,1)} async-done(((bf16[352,2048]{1,0:T(8,128)(2,1)}), bf16[2816,2048]{1,0:T(8,128)(2,1)}) %all-gather.12.cloned.1.call-update) | async-done | bytes 11534352 | tf_op jit(solution)/shard_map/all_gather | solution.py:98
  213.3 6.0 %fusion.58 = (f32[128]{0:T(128)S(1)}, f32[128,2048]{1,0:T(8,128)S(1)}) fusion(bf16[128,2816]{0,1:T(8,128)(2,1)S(1)} %bitcast.148, bf16[2816,2048]{1,0:T(8,128)(2,1)} %all-gather.12.cloned.1.call-done, bf16[128,2048]{1,0:T(8,128)(2,1)S(1)} %copy-done.3), kind=kOutput, calls=%fused_computation.96 | convolution fusion | flops 1477705600 | bytes 13828608 | tf_op jit(solution)/shard_map/dot_general | solution.py:107
  221.7 7.0 %all-to-all-start.3 = ((bf16[16,128,128]{1,2,0:T(8,128)(2,1)}), bf16[16,128,128]{1,2,0:T(8,128)(2,1)S(1)}, u32[]{:S(2)}, u32[]{:S(2)}) async-start(bf16[16,128,128]{1,2,0:T(8,128)(2,1)} %broadcast_in_dim.35), calls=%async_computation.3 | async-start | bytes 1048576 | tf_op jit(solution)/shard_map/all_to_all | solution.py:18
  229.0 17.3 %all-to-all-done.3 = bf16[16,128,128]{1,2,0:T(8,128)(2,1)S(1)} async-done(((bf16[16,128,128]{1,2,0:T(8,128)(2,1)}), bf16[16,128,128]{1,2,0:T(8,128)(2,1)S(1)}, u32[]{:S(2)}, u32[]{:S(2)}) %all-to-all-start.3) | async-done | bytes 524320 | tf_op jit(solution)/shard_map/all_to_all | solution.py:18
  247.2 39.2 %all-gather.16.cloned.1.call-done = bf16[2048,384]{1,0:T(8,128)(2,1)} async-done(((bf16[128,384]{1,0:T(8,128)(2,1)}), bf16[2048,384]{1,0:T(8,128)(2,1)}) %all-gather.16.cloned.1.call-update) | async-done | bytes 1572880 | tf_op jit(solution)/shard_map/all_gather | solution.py:35
  286.4 45.3 %all-gather.14.cloned.1.call-done = bf16[1024,2048]{1,0:T(8,128)(2,1)} async-done(((bf16[128,2048]{1,0:T(8,128)(2,1)}), bf16[1024,2048]{1,0:T(8,128)(2,1)}) %all-gather.14.cloned.1.call-update) | async-done | bytes 4194320 | tf_op jit(solution)/shard_map/all_gather | solution.py:113
  331.8 3.8 fusion.45
  335.7 3.7 fusion.44
  339.7 3.8 fusion.56
  344.0 6.3 %fusion.61 = f32[16,1,64,64]{3,0,1,2:T(8,128)S(1)} fusion(f32[16,1,64,64]{3,0,1,2:T(8,128)S(1)} %copy.47), kind=kOutput, calls=%fused_computation.99 | output fusion | flops 4128768 | bytes 524288 | tf_op jit(solution)/shard_map/jit(cumsum)/reduce_window_sum | solution.py:71
  353.9 30.5 %while.13 = (s32[]{:T(128)}, f32[1,64,128]{2,1,0:T(8,128)S(1)}, f32[16,1,64,128]{3,2,1,0:T(8,128)S(1)}, f32[16,1,64,64]{3,0,1,2:T(8,128)S(1)}, f32[16,1,64,64]{3...) while((s32[]{:T(128)}, f32[1,64,128]{2,1,0:T(8,128)S(1)}, ...), condition=%wide.region_5.6_spmd.clone, body=%wide.region_3.5_spmd.clone.sunk | while | flops 4509699 | bytes 544884 | solution.py:73
  384.7 3.6 fusion.52
  392.8 6.5 %all-to-all-done.2 = bf16[8,128,128]{1,2,0:T(8,128)(2,1)S(1)} async-done(((bf16[8,128,128]{1,2,0:T(8,128)(2,1)}), bf16[8,128,128]{1,2,0:T(8,128)(2,1)S(1)}, u32[]{:S(2)}, u32[]{:S(2)}) %all-to-all-start.2) | async-done | bytes 262176 | tf_op jit(solution)/shard_map/all_to_all | solution.py:141
  399.3 3.8 fusion.59
  404.4 35.0 %all-gather.20.cloned.1.call-done = bf16[1024,2048]{1,0:T(8,128)(2,1)} async-done(((bf16[128,2048]{1,0:T(8,128)(2,1)}), bf16[1024,2048]{1,0:T(8,128)(2,1)}) %all-gather.20.cloned.1.call-update) | async-done | bytes 4194320 | tf_op jit(solution)/shard_map/all_gather | solution.py:101
  439.3 4.5 fusion.38
  443.8 4.6 fusion.34
  448.6 14.7 %all_to_all.68 = bf16[8,128,352]{1,2,0:T(8,128)(2,1)S(1)} all-to-all(bf16[8,128,352]{1,2,0:T(8,128)(2,1)S(1)} %bitcast.150), channel_id=1, replica_groups=mesh['rep'=2,'fs'=16,'tp'=8] {'tp'}, dimensions={0} | all-to-all | bytes 1441792 | tf_op jit(solution)/shard_map/all_to_all | solution.py:106
  (235 shorter events, 55.8 us)
Async XLA Ops:
  6.5 333.1 %copy-start = (bf16[2048,32]{0,1:T(8,128)(2,1)S(1)}, bf16[2048,32]{0,1:T(8,128)(2,1)}, u32[]{:S(2)}) copy-start(bf16[2048,32]{0,1:T(8,128)(2,1)} %param.24) | copy-start | bytes 393220
  6.5 90.5 %all-gather.8.cloned.1.call-start = ((), (), s32[]{:S(2)}) async-start(), calls=%async_computation.5 | async-start | bytes 3063808 | tf_op jit(solution)/shard_map/all_gather | solution.py:35
  8.2 133.7 %all-gather.10.cloned.1.call-start = ((), (), s32[]{:S(2)}) async-start(), calls=%async_computation.6 | async-start | bytes 4718592 | tf_op jit(solution)/shard_map/all_gather | solution.py:101
  9.0 204.3 %all-gather.12.cloned.1.call-start = ((), (), s32[]{:S(2)}) async-start(), calls=%async_computation.7 | async-start | bytes 12976128 | tf_op jit(solution)/shard_map/all_gather | solution.py:98
  67.2 1.6 copy-start.6
  68.6 217.8 %all-gather.16.cloned.1.call-start = ((), (), s32[]{:S(2)}) async-start(), calls=%async_computation.9 | async-start | bytes 1671168 | tf_op jit(solution)/shard_map/all_gather | solution.py:35
  97.0 49.4 %copy-start.14 = (bf16[2048,704]{0,1:T(8,128)(2,1)S(1)}, bf16[2048,704]{0,1:T(8,128)(2,1)}, u32[]{:S(2)}) copy-start(bf16[2048,704]{0,1:T(8,128)(2,1)} %all-gather.8.cloned.1.call-done) | copy-start | bytes 8650756
  141.9 4.5 copy-start.13
  148.3 4.8 %copy-start.8 = (f32[3,2048]{1,0:T(4,128)S(1)}, f32[3,2048]{1,0:T(4,128)}, u32[]{:S(2)}) copy-start(f32[3,2048]{1,0:T(4,128)} %param.29) | copy-start | bytes 73732
  148.3 64.9 %copy-start.3 = (bf16[128,2048]{1,0:T(8,128)(2,1)S(1)}, bf16[128,2048]{1,0:T(8,128)(2,1)}, u32[]{:S(2)}) copy-start(bf16[128,2048]{1,0:T(8,128)(2,1)} %param.16) | copy-start | bytes 1572868
  149.3 18.6 %all-to-all-start = ((bf16[8,128,352]{1,2,0:T(8,128)(2,1)}), bf16[8,128,352]{1,2,0:T(8,128)(2,1)S(1)}, u32[]{:S(2)}, u32[]{:S(2)}) async-start(bf16[8,128,352]{1,2,0:T(8,128)(2,1)} %bitcast.112), calls=%async_computation | async-start | bytes 1441792 | tf_op jit(solution)/shard_map/all_to_all | solution.py:106
  153.1 178.7 %all-gather.14.cloned.1.call-start = ((), (), s32[]{:S(2)}) async-start(), calls=%async_computation.8 | async-start | bytes 4718592 | tf_op jit(solution)/shard_map/all_gather | solution.py:113
  221.7 24.6 %all-to-all-start.3 = ((bf16[16,128,128]{1,2,0:T(8,128)(2,1)}), bf16[16,128,128]{1,2,0:T(8,128)(2,1)S(1)}, u32[]{:S(2)}, u32[]{:S(2)}) async-start(bf16[16,128,128]{1,2,0:T(8,128)(2,1)} %broadcast_in_dim.35), calls=%async_computation.3 | async-start | bytes 1048576 | tf_op jit(solution)/shard_map/all_to_all | solution.py:18
  228.8 164.0 %all-gather.18.cloned.1.call-start = ((), (), s32[]{:S(2)}) async-start(), calls=%async_computation.10 | async-start | bytes 4718592 | tf_op jit(solution)/shard_map/all_gather | solution.py:140
  335.7 4.0 copy-start.11
  335.7 4.0 copy-start.12
  353.9 30.8 %copy-start.15 = (f32[128]{0:T(128)S(1)}, f32[128]{0:T(128)}, u32[]{:S(2)}) copy-start(f32[128]{0:T(128)} %param.27) | copy-start | bytes 1540
  384.7 14.6 %copy-start.1 = (bf16[128,2048]{1,0:T(8,128)(2,1)S(1)}, bf16[128,2048]{1,0:T(8,128)(2,1)}, u32[]{:S(2)}) copy-start(bf16[128,2048]{1,0:T(8,128)(2,1)} %multiply_convert_fusion.2) | copy-start | bytes 1572868
  389.2 10.1 %all-to-all-start.2 = ((bf16[8,128,128]{1,2,0:T(8,128)(2,1)}), bf16[8,128,128]{1,2,0:T(8,128)(2,1)S(1)}, u32[]{:S(2)}, u32[]{:S(2)}) async-start(bf16[8,128,128]{1,2,0:T(8,128)(2,1)} %copy.54), calls=%async_computation.2 | async-start | bytes 524288 | tf_op jit(solution)/shard_map/all_to_all | solution.py:141
  392.8 46.6 %all-gather.20.cloned.1.call-start = ((), (), s32[]{:S(2)}) async-start(), calls=%async_computation.11 | async-start | bytes 4718592 | tf_op jit(solution)/shard_map/all_gather | solution.py:101
  439.3 23.9 %slice-start = ((s8[11534336]{0:T(1024)(128)(4,1)}), s8[4194304]{0:T(1024)(128)(4,1)S(1)}, s32[]{:S(2)}) async-start(s8[11534336]{0:T(1024)(128)(4,1)} %bitcast.141), calls=%async_computation.12 | async-start | bytes 8388608
  439.3 23.9 %slice-start.1 = ((s8[11534336]{0:T(1024)(128)(4,1)}), s8[4194304]{0:T(1024)(128)(4,1)S(1)}, s32[]{:S(2)}) async-start(s8[11534336]{0:T(1024)(128)(4,1)} %bitcast.141), calls=%async_computation.13 | async-start | bytes 8388608
  443.8 19.5 %slice-start.2 = ((s8[11534336]{0:T(1024)(128)(4,1)}), s8[3145728]{0:T(1024)(128)(4,1)S(1)}, s32[]{:S(2)}) async-start(s8[11534336]{0:T(1024)(128)(4,1)} %bitcast.141), calls=%async_computation.14 | async-start | bytes 6291456
  448.4 14.8 %copy-start.2 = (bf16[128,2048]{1,0:T(8,128)(2,1)S(1)}, bf16[128,2048]{1,0:T(8,128)(2,1)}, u32[]{:S(2)}) copy-start(bf16[128,2048]{1,0:T(8,128)(2,1)} %multiply_convert_fusion.1) | copy-start | bytes 1572868
  (5 other events, 6.7 us)
Sparse Core Ops, SparseCore 0:
  9.0 87.9 all-gather.7
  98.9 42.9 all-gather.9
  143.8 69.4 all-gather.11
  214.9 71.4 all-gather.15
  288.1 43.5 all-gather.13
  333.4 38.1 all-gather.17
  404.5 34.8 all-gather.19
where the time goes:
time: 474 us; the launch traced here: 473 us
  waiting for transfers between devices  277 us (58%)
  blocking collectives  71.8 us (15%)
  matrix products  52.6 us (11%)
  other arithmetic  34.7 us (7%)
  starting transfers between devices  14.7 us (3%)
  between operations  13.8 us (3%)
  local copies, waits for them, and re-layouts  8.37 us (2%)
    all_gather x2, waiting for transfers between devices, ffn_half(): gathered = lax.all_gather(current, 'tp', axis=0, tiled=True)  79.9 us
    all_gather x2, waiting for transfers between devices, side_by_side(): result = lax.all_gather(both, axis, axis=dim, tiled=True)  66.6 us
    all_to_all x1, blocking collectives, from_everyone(): return lax.all_to_all(copies, axis, split_axis=0, concat_axis=0, tiled=True)  57.1 us
    all_gather x1, waiting for transfers between devices, on_device(): gathered = lax.all_gather(first, 'tp', axis=0, tiled=True)  45.3 us
    all_gather x1, waiting for transfers between devices, on_device(): down_full = lax.all_gather(down_local, 'tp', axis=0, tiled=True)  45.3 us
    reduce_sum x16, other arithmetic, advance(): jnp.sum(query_blk[:, :, None, :] * key_blk[:, None, :, :] * jnp.exp(log_g...  21.7 us
    all_to_all x1, waiting for transfers between devices, from_everyone(): return lax.all_to_all(copies, axis, split_axis=0, concat_axis=0, tiled=True)  17.3 us
    all_to_all x1, waiting for transfers between devices, ffn_half(): lax.all_to_all(hidden, 'tp', split_axis=0, concat_axis=1, tiled=True)  14.9 us
  transfers between devices with their start and end apart: 10, of which 9 were waited for; matrix products, arithmetic and copies ran while one was open for 16% of the time, Pallas kernels for 0%

commit v1 on v0

--- a/solution.py
+++ b/solution.py
@@ -110,7 +110,12 @@
         )
 
     first = ffn_half(stream, norm_gain[0])
-    gathered = lax.all_gather(first, "tp", axis=0, tiled=True)
+    ring = [first]
+    for hop in range(7):
+        ring.append(lax.ppermute(ring[-1], "tp", [(dev, (dev + 1) % 8) for dev in range(8)]))
+    gathered = jnp.roll(
+        jnp.concatenate(ring[::-1], axis=0), (lax.axis_index("tp") + 1) * ring[0].shape[0], axis=0
+    )
     length = gathered.shape[0]
     pieces = side_by_side((query_weight, key_weight, value_weight, outgate_weight), "fs", 0, 1)
     query, key_rows, value_rows, outgate = tuple(

time: 474 us -> 457 us (0.964)
  waiting for transfers between devices: 277 us -> 213 us
  starting transfers between devices: 14.7 us -> 39.8 us
  local copies, waits for them, and re-layouts: 8.37 us -> 28.6 us
    all_gather x1 -> x0, waiting for transfers between devices: 45.3 us -> none  [on_device(): gathered = lax.all_gather(first, 'tp', axis=0, tiled=True)]
    all_gather x2, waiting for transfers between devices: 66.6 us -> 28.5 us  [side_by_side(): result = lax.all_gather(both, axis, axis=dim, tiled=True)]
    ppermute x0 -> x7, waiting for transfers between devices: none -> 30.1 us  [on_device(): lax.ppermute(ring[-1], 'tp', [(dev, (dev + 1) % 8) for dev in range(8)])]
    unnamed x43 -> x65, local copies, waits for them, and re-layouts: 1.67 us -> 22 us
    ppermute x0 -> x7, starting transfers between devices: none -> 12.6 us  [on_device(): lax.ppermute(ring[-1], 'tp', [(dev, (dev + 1) % 8) for dev in range(8)])]
    all_to_all x1, starting transfers between devices: 3.58 us -> 16.1 us  [on_device(): lax.all_to_all(gated, 'tp', split_axis=0, concat_axis=1, tiled=True)]
    all_to_all x1, waiting for transfers between devices: 17.3 us -> 10.5 us  [from_everyone(): return lax.all_to_all(copies, axis, split_axis=0, concat_axis=0, tiled=True)]
  transfers between devices with their start and end apart: 10 -> 16, of which waited for: 9 -> 12; matrix products, arithmetic and copies ran while one was open for 16% -> 20% of each run, Pallas kernels for 0% -> 0%
where the time goes in v1:
time: 457 us; the launch traced here: 456 us
  waiting for transfers between devices  213 us (47%)
  blocking collectives  71.7 us (16%)
  matrix products  52.7 us (12%)
  starting transfers between devices  39.8 us (9%)
  other arithmetic  35.9 us (8%)
  local copies, waits for them, and re-layouts  28.6 us (6%)
  between operations  13.8 us (3%)
    all_gather x2, waiting for transfers between devices, ffn_half(): gathered = lax.all_gather(current, 'tp', axis=0, tiled=True)  76.3 us
    all_to_all x1, blocking collectives, from_everyone(): return lax.all_to_all(copies, axis, split_axis=0, concat_axis=0, tiled=True)  57.1 us
    all_gather x1, waiting for transfers between devices, on_device(): down_full = lax.all_gather(down_local, 'tp', axis=0, tiled=True)  45.1 us
    ppermute x7, waiting for transfers between devices, on_device(): lax.ppermute(ring[-1], 'tp', [(dev, (dev + 1) % 8) for dev in range(8)])  30.1 us
    all_gather x2, waiting for transfers between devices, side_by_side(): result = lax.all_gather(both, axis, axis=dim, tiled=True)  28.5 us
    unnamed x65, local copies, waits for them, and re-layouts  22 us
    reduce_sum x16, other arithmetic, advance(): jnp.sum(query_blk[:, :, None, :] * key_blk[:, None, :, :] * jnp.exp(log_g...  21.7 us
    all_to_all x1, starting transfers between devices, on_device(): lax.all_to_all(gated, 'tp', split_axis=0, concat_axis=1, tiled=True)  16.1 us
  transfers between devices with their start and end apart: 16, of which 12 were waited for; matrix products, arithmetic and copies ran while one was open for 20% of the time, Pallas kernels for 0%

profile of v1, /device:TPU:1, one launch (start us, length us, event | category | flops | bytes accessed | tf_op | source)
XLA Modules:
  0.0 456.0 jit_solution(3742335174867696491)
XLA Ops:
  10.1 57.1 %all_to_all.67 = bf16[16,352,128]{2,1,0:T(8,128)(2,1)S(1)} all-to-all(bf16[16,352,128]{2,1,0:T(8,128)(2,1)S(1)} %broadcast_in_dim.32), channel_id=1, replica_groups=mesh['rep'=2,'fs'=16,'tp'=8] {'fs'}, dimensions={0} | all-to-all | bytes 2883584 | tf_op jit(solution)/shard_map/all_to_all | solution.py:18
  68.5 28.5 %all-gather.7.cloned.1.call-done = bf16[2048,704]{0,1:T(8,128)(2,1)} async-done(((bf16[128,704]{0,1:T(8,128)(2,1)}), bf16[2048,704]{0,1:T(8,128)(2,1)}) %all-gather.7.cloned.1.call-update) | async-done | bytes 2883600 | tf_op jit(solution)/shard_map/all_gather | solution.py:35
  97.0 44.9 %all-gather.9.cloned.1.call-done = bf16[1024,2048]{1,0:T(8,128)(2,1)} async-done(((bf16[128,2048]{1,0:T(8,128)(2,1)}), bf16[1024,2048]{1,0:T(8,128)(2,1)}) %all-gather.9.cloned.1.call-update) | async-done | bytes 4194320 | tf_op jit(solution)/shard_map/all_gather | solution.py:101
  141.9 4.5 convolution_bitcast_fusion.2
  153.3 15.1 %all-to-all-done = bf16[8,128,352]{1,2,0:T(8,128)(2,1)S(1)} async-done(((bf16[8,128,352]{1,2,0:T(8,128)(2,1)}), bf16[8,128,352]{1,2,0:T(8,128)(2,1)S(1)}, u32[]{:S(2)}, u32[]{:S(2)}) %all-to-all-start) | async-done | bytes 720928 | tf_op jit(solution)/shard_map/all_to_all | solution.py:106
  168.4 45.1 %all-gather.11.cloned.1.call-done = bf16[2816,2048]{1,0:T(8,128)(2,1)} async-done(((bf16[352,2048]{1,0:T(8,128)(2,1)}), bf16[2816,2048]{1,0:T(8,128)(2,1)}) %all-gather.11.cloned.1.call-update) | async-done | bytes 11534352 | tf_op jit(solution)/shard_map/all_gather | solution.py:98
  213.5 6.1 %fusion.103 = (f32[128]{0:T(128)S(1)}, f32[128,2048]{1,0:T(8,128)S(1)}) fusion(bf16[128,2816]{0,1:T(8,128)(2,1)S(1)} %bitcast.143, bf16[2816,2048]{1,0:T(8,128)(2,1)} %all-gather.11.cloned.1.call-done, bf16[128,2048]{1,0:T(8,128)(2,1)S(1)} %copy-done.2), kind=kOutput, calls=%fused_computation.127 | convolution fusion | flops 1477705600 | bytes 13828608 | tf_op jit(solution)/shard_map/dot_general | solution.py:107
  220.1 6.1 %collective-permute-done = bf16[128,2048]{1,0:T(8,128)(2,1)S(1)} collective-permute-done((bf16[128,2048]{1,0:T(8,128)(2,1)S(1)}, bf16[128,2048]{1,0:T(8,128)(2,1)S(1)}, u32[]{:S(2)}, u32[]{:S(2)}) %collective-permute-start) | collective-permute-done | bytes 524320 | tf_op jit(solution)/shard_map/ppermute | solution.py:115
  229.7 5.1 %collective-permute-done.1 = bf16[128,2048]{1,0:T(8,128)(2,1)S(1)} collective-permute-done((bf16[128,2048]{1,0:T(8,128)(2,1)S(1)}, bf16[128,2048]{1,0:T(8,128)(2,1)S(1)}, u32[]{:S(2)}, u32[]{:S(2)}) %collective-permute-start.1) | collective-permute-done | bytes 524320 | tf_op jit(solution)/shard_map/ppermute | solution.py:115
  237.3 6.1 %collective-permute-done.2 = bf16[128,2048]{1,0:T(8,128)(2,1)S(1)} collective-permute-done((bf16[128,2048]{1,0:T(8,128)(2,1)S(1)}, bf16[128,2048]{1,0:T(8,128)(2,1)S(1)}, u32[]{:S(2)}, u32[]{:S(2)}) %collective-permute-start.2) | collective-permute-done | bytes 524320 | tf_op jit(solution)/shard_map/ppermute | solution.py:115
  245.9 6.1 %collective-permute-done.3 = bf16[128,2048]{1,0:T(8,128)(2,1)S(1)} collective-permute-done((bf16[128,2048]{1,0:T(8,128)(2,1)S(1)}, bf16[128,2048]{1,0:T(8,128)(2,1)S(1)}, u32[]{:S(2)}, u32[]{:S(2)}) %collective-permute-start.3) | collective-permute-done | bytes 524320 | tf_op jit(solution)/shard_map/ppermute | solution.py:115
  255.4 6.6 %collective-permute-done.4 = bf16[128,2048]{1,0:T(8,128)(2,1)} collective-permute-done((bf16[128,2048]{1,0:T(8,128)(2,1)S(1)}, bf16[128,2048]{1,0:T(8,128)(2,1)}, u32[]{:S(2)}, u32[]{:S(2)}) %collective-permute-start.4) | collective-permute-done | bytes 524320 | tf_op jit(solution)/shard_map/ppermute | solution.py:115
  265.1 7.0 %all-to-all-start.3 = ((bf16[16,128,128]{1,2,0:T(8,128)(2,1)}), bf16[16,128,128]{1,2,0:T(8,128)(2,1)S(1)}, u32[]{:S(2)}, u32[]{:S(2)}) async-start(bf16[16,128,128]{1,2,0:T(8,128)(2,1)} %broadcast_in_dim.35), calls=%async_computation.3 | async-start | bytes 1048576 | tf_op jit(solution)/shard_map/all_to_all | solution.py:18
  273.0 10.5 %all-to-all-done.3 = bf16[16,128,128]{1,2,0:T(8,128)(2,1)S(1)} async-done(((bf16[16,128,128]{1,2,0:T(8,128)(2,1)}), bf16[16,128,128]{1,2,0:T(8,128)(2,1)S(1)}, u32[]{:S(2)}, u32[]{:S(2)}) %all-to-all-start.3) | async-done | bytes 524320 | tf_op jit(solution)/shard_map/all_to_all | solution.py:18
  309.9 6.3 %fusion.106 = f32[16,1,64,64]{3,0,1,2:T(8,128)S(1)} fusion(f32[16,1,64,64]{3,0,1,2:T(8,128)S(1)} %copy.47), kind=kOutput, calls=%fused_computation.130 | output fusion | flops 4128768 | bytes 524288 | tf_op jit(solution)/shard_map/jit(cumsum)/reduce_window_sum | solution.py:71
  316.3 3.8 fusion.64
  327.9 30.5 %while.13 = (s32[]{:T(128)}, f32[1,64,128]{2,1,0:T(8,128)S(1)}, f32[16,1,64,128]{3,2,1,0:T(8,128)S(1)}, f32[16,1,64,64]{3,0,1,2:T(8,128)S(1)}, f32[16,1,64,64]{3...) while((s32[]{:T(128)}, f32[1,64,128]{2,1,0:T(8,128)S(1)}, ...), condition=%wide.region_5.6_spmd.clone, body=%wide.region_3.5_spmd.clone.sunk | while | flops 4509699 | bytes 544884 | solution.py:73
  363.2 16.1 %all-to-all-start.2 = ((bf16[8,128,128]{1,2,0:T(8,128)(2,1)}), bf16[8,128,128]{1,2,0:T(8,128)(2,1)S(1)}, u32[]{:S(2)}, u32[]{:S(2)}) async-start(bf16[8,128,128]{1,2,0:T(8,128)(2,1)} %copy.54), calls=%async_computation.2 | async-start | bytes 524288 | tf_op jit(solution)/shard_map/all_to_all | solution.py:146
  379.3 6.5 %all-to-all-done.2 = bf16[8,128,128]{1,2,0:T(8,128)(2,1)S(1)} async-done(((bf16[8,128,128]{1,2,0:T(8,128)(2,1)}), bf16[8,128,128]{1,2,0:T(8,128)(2,1)S(1)}, u32[]{:S(2)}, u32[]{:S(2)}) %all-to-all-start.2) | async-done | bytes 262176 | tf_op jit(solution)/shard_map/all_to_all | solution.py:146
  385.8 3.8 fusion.104
  390.9 31.5 %all-gather.17.cloned.1.call-done = bf16[1024,2048]{1,0:T(8,128)(2,1)} async-done(((bf16[128,2048]{1,0:T(8,128)(2,1)}), bf16[1024,2048]{1,0:T(8,128)(2,1)}) %all-gather.17.cloned.1.call-update) | async-done | bytes 4194320 | tf_op jit(solution)/shard_map/all_gather | solution.py:101
  422.3 4.5 fusion.48
  426.8 4.6 %fusion.44 = bf16[44,8,8,128]{3,2,1,0:T(8,128)(2,1)S(1)} fusion(bf16[1024,2048]{1,0:T(8,128)(2,1)} %all-gather.17.cloned.1.call-done, f32[1024,352]{0,1:T(8,128)S(1)} %fusion.48, bf16[2048,704]{0,1:T(8,128)(2,1)} %all-gather.7.cloned.1.call-done), kind=kOutput, calls=%fused_computation.58 | convolution fusion | flops 1478557696 | bytes 7798784 | tf_op jit(solution)/shard_map/dot_general | solution.py:104
  431.6 14.5 %all_to_all.68 = bf16[8,128,352]{1,2,0:T(8,128)(2,1)S(1)} all-to-all(bf16[8,128,352]{1,2,0:T(8,128)(2,1)S(1)} %bitcast.145), channel_id=1, replica_groups=mesh['rep'=2,'fs'=16,'tp'=8] {'tp'}, dimensions={0} | all-to-all | bytes 1441792 | tf_op jit(solution)/shard_map/all_to_all | solution.py:106
  (270 shorter events, 101.1 us)
Async XLA Ops:
  6.5 299.1 %copy-start = (bf16[2048,32]{0,1:T(8,128)(2,1)S(1)}, bf16[2048,32]{0,1:T(8,128)(2,1)}, u32[]{:S(2)}) copy-start(bf16[2048,32]{0,1:T(8,128)(2,1)} %param.24) | copy-start | bytes 393220
  6.5 90.5 %all-gather.7.cloned.1.call-start = ((), (), s32[]{:S(2)}) async-start(), calls=%async_computation.5 | async-start | bytes 3063808 | tf_op jit(solution)/shard_map/all_gather | solution.py:35
  8.2 133.7 %all-gather.9.cloned.1.call-start = ((), (), s32[]{:S(2)}) async-start(), calls=%async_computation.6 | async-start | bytes 4718592 | tf_op jit(solution)/shard_map/all_gather | solution.py:101
  9.0 204.5 %all-gather.11.cloned.1.call-start = ((), (), s32[]{:S(2)}) async-start(), calls=%async_computation.7 | async-start | bytes 12976128 | tf_op jit(solution)/shard_map/all_gather | solution.py:98
  146.7 66.8 %copy-start.2 = (bf16[128,2048]{1,0:T(8,128)(2,1)S(1)}, bf16[128,2048]{1,0:T(8,128)(2,1)}, u32[]{:S(2)}) copy-start(bf16[128,2048]{1,0:T(8,128)(2,1)} %param.16) | copy-start | bytes 1572868
  149.5 18.8 %all-to-all-start = ((bf16[8,128,352]{1,2,0:T(8,128)(2,1)}), bf16[8,128,352]{1,2,0:T(8,128)(2,1)S(1)}, u32[]{:S(2)}, u32[]{:S(2)}) async-start(bf16[8,128,352]{1,2,0:T(8,128)(2,1)} %bitcast.107), calls=%async_computation | async-start | bytes 1441792 | tf_op jit(solution)/shard_map/all_to_all | solution.py:106
  153.2 163.0 %all-gather.13.cloned.1.call-start = ((), (), s32[]{:S(2)}) async-start(), calls=%async_computation.8 | async-start | bytes 1671168 | tf_op jit(solution)/shard_map/all_gather | solution.py:35
  213.5 50.6 %copy-start.11 = (bf16[128,128]{1,0:T(8,128)(2,1)S(1)}, bf16[128,128]{1,0:T(8,128)(2,1)}, u32[]{:S(2)}) copy-start(bf16[128,128]{1,0:T(8,128)(2,1)} %param.28) | copy-start | bytes 98308
  220.1 6.1 %collective-permute-start = (bf16[128,2048]{1,0:T(8,128)(2,1)S(1)}, bf16[128,2048]{1,0:T(8,128)(2,1)S(1)}, u32[]{:S(2)}, u32[]{:S(2)}) collective-permute-start(bf16[128,2048]{1,0:T(8,128)(2,1)S(1)} %multiply_convert_fusion.2), channel_id=1, source_target_pairs={{0,1},{1,2},{2,3},{3,4},{4,5},{5,6},{6,7},{7,0},{8,9},{9,10},{10,1... | collective-permute-start | bytes 1572872 | tf_op jit(solution)/shard_map/ppermute | solution.py:115
  226.2 8.6 %collective-permute-start.1 = (bf16[128,2048]{1,0:T(8,128)(2,1)S(1)}, bf16[128,2048]{1,0:T(8,128)(2,1)S(1)}, u32[]{:S(2)}, u32[]{:S(2)}) collective-permute-start(bf16[128,2048]{1,0:T(8,128)(2,1)S(1)} %collective-permute-done), channel_id=1, source_target_pairs={{0,1},{1,2},{2,3},{3,4},{4,5},{5,6},{6,7},{7,0},{8,9},{9,10},{10,1... | collective-permute-start | bytes 1572872 | tf_op jit(solution)/shard_map/ppermute | solution.py:115
  234.8 8.6 %collective-permute-start.2 = (bf16[128,2048]{1,0:T(8,128)(2,1)S(1)}, bf16[128,2048]{1,0:T(8,128)(2,1)S(1)}, u32[]{:S(2)}, u32[]{:S(2)}) collective-permute-start(bf16[128,2048]{1,0:T(8,128)(2,1)S(1)} %collective-permute-done.1), channel_id=1, source_target_pairs={{0,1},{1,2},{2,3},{3,4},{4,5},{5,6},{6,7},{7,0},{8,9},{9,10},{10,1... | collective-permute-start | bytes 1572872 | tf_op jit(solution)/shard_map/ppermute | solution.py:115
  243.4 21.7 %copy-start.4 = (bf16[128,2048]{1,0:T(8,128)(2,1)}, bf16[128,2048]{1,0:T(8,128)(2,1)S(1)}, u32[]{:S(2)}) copy-start(bf16[128,2048]{1,0:T(8,128)(2,1)S(1)} %collective-permute-done.2) | copy-start | bytes 1572868
  243.4 8.6 %collective-permute-start.3 = (bf16[128,2048]{1,0:T(8,128)(2,1)S(1)}, bf16[128,2048]{1,0:T(8,128)(2,1)S(1)}, u32[]{:S(2)}, u32[]{:S(2)}) collective-permute-start(bf16[128,2048]{1,0:T(8,128)(2,1)S(1)} %collective-permute-done.2), channel_id=1, source_target_pairs={{0,1},{1,2},{2,3},{3,4},{4,5},{5,6},{6,7},{7,0},{8,9},{9,10},{10,1... | collective-permute-start | bytes 1572872 | tf_op jit(solution)/shard_map/ppermute | solution.py:115
  252.9 9.1 %collective-permute-start.4 = (bf16[128,2048]{1,0:T(8,128)(2,1)S(1)}, bf16[128,2048]{1,0:T(8,128)(2,1)}, u32[]{:S(2)}, u32[]{:S(2)}) collective-permute-start(bf16[128,2048]{1,0:T(8,128)(2,1)S(1)} %collective-permute-done.3), channel_id=1, source_target_pairs={{0,1},{1,2},{2,3},{3,4},{4,5},{5,6},{6,7},{7,0},{8,9},{9,10},{10,1... | collective-permute-start | bytes 1572872 | tf_op jit(solution)/shard_map/ppermute | solution.py:115
  262.0 10.4 %collective-permute-start.5 = (bf16[128,2048]{1,0:T(8,128)(2,1)}, bf16[128,2048]{1,0:T(8,128)(2,1)}, u32[]{:S(2)}, u32[]{:S(2)}) collective-permute-start(bf16[128,2048]{1,0:T(8,128)(2,1)} %collective-permute-done.4), channel_id=1, source_target_pairs={{0,1},{1,2},{2,3},{3,4},{4,5},{5,6},{6,7},{7,0},{8,9},{9,10},{10,1... | collective-permute-start | bytes 1572872 | tf_op jit(solution)/shard_map/ppermute | solution.py:115
  265.1 18.4 %all-to-all-start.3 = ((bf16[16,128,128]{1,2,0:T(8,128)(2,1)}), bf16[16,128,128]{1,2,0:T(8,128)(2,1)S(1)}, u32[]{:S(2)}, u32[]{:S(2)}) async-start(bf16[16,128,128]{1,2,0:T(8,128)(2,1)} %broadcast_in_dim.35), calls=%async_computation.3 | async-start | bytes 1048576 | tf_op jit(solution)/shard_map/all_to_all | solution.py:18
  272.2 107.1 %all-gather.15.cloned.1.call-start = ((), (), s32[]{:S(2)}) async-start(), calls=%async_computation.9 | async-start | bytes 4718592 | tf_op jit(solution)/shard_map/all_gather | solution.py:145
  272.4 12.0 %collective-permute-start.6 = (bf16[128,2048]{1,0:T(8,128)(2,1)}, bf16[128,2048]{1,0:T(8,128)(2,1)}, u32[]{:S(2)}, u32[]{:S(2)}) collective-permute-start(bf16[128,2048]{1,0:T(8,128)(2,1)} %collective-permute-done.5), channel_id=1, source_target_pairs={{0,1},{1,2},{2,3},{3,4},{4,5},{5,6},{6,7},{7,0},{8,9},{9,10},{10,1... | collective-permute-start | bytes 1572872 | tf_op jit(solution)/shard_map/ppermute | solution.py:115
  327.9 30.8 %copy-start.19 = (f32[128]{0:T(128)S(1)}, f32[128]{0:T(128)}, u32[]{:S(2)}) copy-start(f32[128]{0:T(128)} %param.27) | copy-start | bytes 1540
  363.2 22.6 %all-to-all-start.2 = ((bf16[8,128,128]{1,2,0:T(8,128)(2,1)}), bf16[8,128,128]{1,2,0:T(8,128)(2,1)S(1)}, u32[]{:S(2)}, u32[]{:S(2)}) async-start(bf16[8,128,128]{1,2,0:T(8,128)(2,1)} %copy.54), calls=%async_computation.2 | async-start | bytes 524288 | tf_op jit(solution)/shard_map/all_to_all | solution.py:146
  379.3 43.0 %all-gather.17.cloned.1.call-start = ((), (), s32[]{:S(2)}) async-start(), calls=%async_computation.10 | async-start | bytes 4718592 | tf_op jit(solution)/shard_map/all_gather | solution.py:101
  422.3 23.8 %slice-start = ((s8[11534336]{0:T(1024)(128)(4,1)}), s8[4194304]{0:T(1024)(128)(4,1)S(1)}, s32[]{:S(2)}) async-start(s8[11534336]{0:T(1024)(128)(4,1)} %bitcast.136), calls=%async_computation.11 | async-start | bytes 8388608
  422.3 23.8 %slice-start.1 = ((s8[11534336]{0:T(1024)(128)(4,1)}), s8[4194304]{0:T(1024)(128)(4,1)S(1)}, s32[]{:S(2)}) async-start(s8[11534336]{0:T(1024)(128)(4,1)} %bitcast.136), calls=%async_computation.12 | async-start | bytes 8388608
  426.8 19.3 %slice-start.2 = ((s8[11534336]{0:T(1024)(128)(4,1)}), s8[3145728]{0:T(1024)(128)(4,1)S(1)}, s32[]{:S(2)}) async-start(s8[11534336]{0:T(1024)(128)(4,1)} %bitcast.136), calls=%async_computation.13 | async-start | bytes 6291456
  (15 other events, 135.6 us)
Sparse Core Ops, SparseCore 0:
  9.0 87.9 all-gather.6
  98.9 42.9 all-gather.8
  143.8 69.6 all-gather.10
  229.9 74.3 all-gather.12
  305.9 47.0 all-gather.14
  391.0 31.2 all-gather.16
